TPU v7x, 32 devices: a whole 2x2x4 slice. The times are simulated.
32 devices in a mesh: kv: 8 (over z, y), tp: 4 (over x, core).
Axes of the slice: x: 2, y: 2, z: 4, core: 2. Of those that a mesh axis runs over, the one named last changes fastest.
Arguments:
- tokens: bfloat16 [32, 4096], P(None, 'kv'), may hold values from -8 to 8, as said below
- attn_gain: float32 [4096], P('kv'), may hold values from 0.1 to 1.9
- query_weight: bfloat16 [4096, 1024], P('kv', 'tp'), may hold values from -0.09375 to 0.09375
- key_weight: bfloat16 [4096, 1024], P('kv', 'tp'), may hold values from -0.09375 to 0.09375
- value_weight: bfloat16 [4096, 2048], P('kv', 'tp'), may hold values from -0.09375 to 0.09375
- outgate_weight: bfloat16 [4096, 2048], P('kv', 'tp'), may hold values from -0.09375 to 0.09375
- code_weight: bfloat16 [4096, 16], P('kv'), may hold values from -0.09375 to 0.09375
- decay_weight: bfloat16 [16, 1024], P(None, 'tp'), may hold values from -6 to 6
- decay_bias: float32 [1024], P('tp'), may hold values from -4 to 2
- head_gain: float32 [256], replicated, may hold values from 0.1 to 1.9
- key_cache: bfloat16 [32, 64, 8, 128], P('kv', None, 'tp'), may hold values from -6 to 6
- value_cache: bfloat16 [32, 64, 8, 256], P('kv', None, 'tp'), may hold values from -6 to 6
- decay_cache: float32 [32, 64, 8, 128], P('kv', None, 'tp'), may hold values from -1.1 to 0
- carried_state: float32 [32, 8, 128, 256], P('kv', 'tp'), may hold values from -24 to 24
- lengths: int32 [32], P('kv'), may hold values from 1 to 64, 832 in all
- output_weight: bfloat16 [2048, 4096], P('tp', 'kv'), may hold values from -0.125 to 0.125
- mlp_gain: float32 [4096], P('kv'), may hold values from 0.1 to 1.9
- gate_weight: bfloat16 [4096, 11008], P('kv', 'tp'), may hold values from -0.09375 to 0.09375
- up_weight: bfloat16 [4096, 11008], P('kv', 'tp'), may hold values from -0.09375 to 0.09375
- down_weight: bfloat16 [11008, 4096], P('tp', 'kv'), may hold values from -0.0546875 to 0.0546875
Outputs:
- layer_out: bfloat16 [32, 4096], P(None, 'kv')
- new_keys: bfloat16 [32, 8, 128], P('kv', 'tp')
- new_values: bfloat16 [32, 8, 256], P('kv', 'tp')
Inputs may be any that keep to these rules, and one draw needn't show every extreme that they name: `tokens`: the features of a row have unlike scales. Sequence b's new token comes right after its lengths[b] live positions; positions from lengths[b] on take no part.
All inputs are finite; a program needn't handle non-finite values. No bound on the sum of `lengths` on one device may be relied on, other than what follows from the above.
Results may differ from a plain program's by a relative error of at most 0.025.
Values may be sent and summed in bfloat16 or wider, within the bound.
A program may use at most 64 MiB of HBM per device.

v0:
```python
import jax
import jax.numpy as jnp
from jax import lax
from jax.sharding import PartitionSpec as P

WIDTH = 4096
EPS = 1e-06
GATE_TEMP = 16.0


def across_heads(partial_value):
    return lax.psum(partial_value.astype(jnp.bfloat16), "tp").astype(jnp.float32)


def block_attention(
    queries,
    new_keys,
    new_values,
    new_decay,
    key_cache,
    value_cache,
    decay_cache,
    carried_state,
    lengths,
):
    positions = jnp.arange(key_cache.shape[1], dtype=jnp.int32)
    live_mask = positions[None, :] < lengths[:, None]
    kept_decay = jnp.where(live_mask[:, :, None, None], decay_cache, jnp.zeros_like(decay_cache))
    later_sum = lax.cumsum(kept_decay, axis=1, reverse=True) - kept_decay
    total_decay = jnp.sum(kept_decay, axis=1)
    decayed = queries.astype(jnp.float32) * jnp.exp(new_decay)
    carried = jnp.einsum(
        "bhd,bhde->bhe",
        decayed * jnp.exp(total_decay),
        carried_state,
        precision=lax.Precision.HIGHEST,
    )
    keyed_cache = key_cache.astype(jnp.float32) * jnp.exp(later_sum)
    scores = jnp.einsum("bhd,bshd->bhs", decayed, keyed_cache, precision=lax.Precision.HIGHEST)
    scores = jnp.where(live_mask[:, None, :], scores, jnp.zeros_like(scores)).astype(jnp.bfloat16)
    within = jnp.einsum("bhs,bshe->bhe", scores, value_cache, preferred_element_type=jnp.float32)
    own_score = jnp.sum(queries.astype(jnp.float32) * new_keys.astype(jnp.float32), axis=-1)
    return carried + within + own_score[..., None] * new_values.astype(jnp.float32)


def mixer_hidden(gate_sum, up_sum, square_sum):
    inv_mid = lax.rsqrt(square_sum / WIDTH + EPS)[:, None]
    return (jax.nn.silu(gate_sum * inv_mid) * (up_sum * inv_mid)).astype(jnp.bfloat16)


def on_device(
    tokens,
    attn_gain,
    query_weight,
    key_weight,
    value_weight,
    outgate_weight,
    code_weight,
    decay_weight,
    decay_bias,
    head_gain,
    key_cache,
    value_cache,
    decay_cache,
    carried_state,
    lengths,
    output_weight,
    mlp_gain,
    gate_weight,
    up_weight,
    down_weight,
):
    local_seqs, heads_here, key_dim, value_dim = carried_state.shape
    token_f = tokens.astype(jnp.float32)
    scaled = (token_f * attn_gain[None, :]).astype(jnp.bfloat16)
    query_part = jnp.dot(scaled, query_weight, preferred_element_type=jnp.float32)
    key_part = jnp.dot(scaled, key_weight, preferred_element_type=jnp.float32)
    value_part = jnp.dot(scaled, value_weight, preferred_element_type=jnp.float32)
    outgate_part = jnp.dot(scaled, outgate_weight, preferred_element_type=jnp.float32)
    code_part = jnp.dot(scaled, code_weight, preferred_element_type=jnp.float32)
    token_squares = jnp.sum(token_f * token_f, axis=1)
    query_sum, key_sum, value_sum, outgate_sum, code_sum, square_sum = (
        lax.psum_scatter(
            query_part.astype(jnp.bfloat16), "kv", scatter_dimension=0, tiled=True
        ).astype(jnp.float32),
        lax.psum_scatter(
            key_part.astype(jnp.bfloat16), "kv", scatter_dimension=0, tiled=True
        ).astype(jnp.float32),
        lax.psum_scatter(
            value_part.astype(jnp.bfloat16), "kv", scatter_dimension=0, tiled=True
        ).astype(jnp.float32),
        lax.psum_scatter(
            outgate_part.astype(jnp.bfloat16), "kv", scatter_dimension=0, tiled=True
        ).astype(jnp.float32),
        lax.psum_scatter(
            code_part.astype(jnp.bfloat16), "kv", scatter_dimension=0, tiled=True
        ).astype(jnp.float32),
        lax.psum_scatter(
            token_squares.astype(jnp.bfloat16), "kv", scatter_dimension=0, tiled=True
        ).astype(jnp.float32),
    )
    inv_rms = lax.rsqrt(square_sum / WIDTH + EPS)[:, None]
    queries = (
        (query_sum * inv_rms * key_dim ** (-0.5))
        .astype(jnp.bfloat16)
        .reshape(local_seqs, heads_here, key_dim)
    )
    new_keys = (key_sum * inv_rms).astype(jnp.bfloat16).reshape(local_seqs, heads_here, key_dim)
    new_values = (
        (value_sum * inv_rms).astype(jnp.bfloat16).reshape(local_seqs, heads_here, value_dim)
    )
    out_gate = (
        (outgate_sum * inv_rms).astype(jnp.bfloat16).reshape(local_seqs, heads_here, value_dim)
    )
    gate_code = (code_sum * inv_rms).astype(jnp.bfloat16)
    pre_gate = (
        jnp.dot(gate_code, decay_weight, preferred_element_type=jnp.float32) + decay_bias[None, :]
    )
    new_decay = (jax.nn.log_sigmoid(pre_gate) / GATE_TEMP).reshape(local_seqs, heads_here, key_dim)
    mixed_heads = block_attention(
        queries,
        new_keys,
        new_values,
        new_decay,
        key_cache,
        value_cache,
        decay_cache,
        carried_state,
        lengths,
    )
    normed = (
        mixed_heads
        * lax.rsqrt(jnp.mean(mixed_heads * mixed_heads, axis=-1, keepdims=True) + EPS)
        * head_gain
    )
    heads_out = (
        (normed * jax.nn.silu(out_gate.astype(jnp.float32)))
        .astype(jnp.bfloat16)
        .reshape(local_seqs, heads_here * value_dim)
    )
    attended = across_heads(
        jnp.dot(
            lax.all_gather(heads_out, "kv", axis=0, tiled=True),
            output_weight,
            preferred_element_type=jnp.float32,
        )
    )
    middle = (token_f + attended).astype(jnp.bfloat16)
    mid_f = middle.astype(jnp.float32)
    scaled_mid = (mid_f * mlp_gain[None, :]).astype(jnp.bfloat16)
    gate_part = jnp.dot(scaled_mid, gate_weight, preferred_element_type=jnp.float32)
    up_part = jnp.dot(scaled_mid, up_weight, preferred_element_type=jnp.float32)
    mid_squares = jnp.sum(mid_f * mid_f, axis=1)
    gate_sum, up_sum, mid_sum = (
        lax.psum(gate_part.astype(jnp.bfloat16), "kv").astype(jnp.float32),
        lax.psum(up_part.astype(jnp.bfloat16), "kv").astype(jnp.float32),
        lax.psum(mid_squares.astype(jnp.bfloat16), "kv").astype(jnp.float32),
    )
    hidden = mixer_hidden(gate_sum, up_sum, mid_sum)
    lifted_part = jnp.dot(hidden, down_weight, preferred_element_type=jnp.float32)
    layer_out = (mid_f + across_heads(lifted_part)).astype(jnp.bfloat16)
    return (layer_out, new_keys, new_values)


def solution(mesh):
    in_specs = (
        P(None, "kv"),
        P("kv"),
        P("kv", "tp"),
        P("kv", "tp"),
        P("kv", "tp"),
        P("kv", "tp"),
        P("kv", None),
        P(None, "tp"),
        P("tp"),
        P(),
        P("kv", None, "tp", None),
        P("kv", None, "tp", None),
        P("kv", None, "tp", None),
        P("kv", "tp", None, None),
        P("kv"),
        P("tp", "kv"),
        P("kv"),
        P("kv", "tp"),
        P("kv", "tp"),
        P("tp", "kv"),
    )
    out_specs = (P(None, "kv"), P("kv", "tp", None), P("kv", "tp", None))
    return jax.shard_map(
        on_device, mesh=mesh, in_specs=in_specs, out_specs=out_specs, check_vma=False
    )
```

profile of v0, /device:TPU:0, one launch (start us, length us, event | category | flops | bytes accessed | tf_op | source)
XLA Modules:
  0.0 236.8 jit_solution(11415016828430029316)
XLA Ops:
  7.3 1.5 fusion.11
  8.8 1.5 convolution_convert_fusion.8
  10.3 1.7 convolution_convert_fusion.7
  12.1 1.7 convolution_convert_fusion.6
  13.8 1.9 convolution_convert_fusion.5
  15.7 1.9 convolution_convert_fusion.4
  18.4 1.2 dynamic-slice
  20.3 2.6 %exponential_multiply_fusion = f32[4,64,2,128]{3,2,1,0:T(2,128)S(1)} fusion(bf16[4,64,2,128]{3,2,1,0:T(2,128)(2,1)} %param.30, f32[4,64,2,128]{3,2,1,0:T(2,128)} %param.32, pred[4,64]{1,0:T(4,128)(4,1)S(1)} %iota_compare_fusion), kind=kOutput, calls=%fused_computation.16 | output fusion | flops 4456448 | bytes 655616 | tf_op jit(solution)/shard_map/block_attention/reduce_window_sum | solution.py:29
  23.2 68.5 %all-reduce.11.cloned.1.call-done = (bf16[32,512]{1,0:T(8,128)(2,1)}, bf16[32]{0:T(256)(128)(2,1)}, bf16[32,256]{1,0:T(8,128)(2,1)}, bf16[32,16]{1,0:T(8,128)(2,...) async-done(((bf16[32,512]{1,0:T(8,128)(2,1)}, bf16[32]{0:T(256)(128)(2,1)}, bf16[32,256]{1,0:T(8,128)(2,1)}, bf16[32,16]{1,0:T(8,128)(2,1)}, ...) | async-done | bytes 99408
  91.8 0.7 fusion.36
  92.5 0.9 fusion.29
  93.4 0.8 multiply_convert_fusion.4
  94.2 0.8 multiply_convert_fusion.3
  95.6 1.8 fusion.41
  97.5 1.1 fusion.1
  98.9 30.6 %all-gather = bf16[8,4,512]{2,1,0:T(4,128)(2,1)S(1)} all-gather(bf16[1,4,512]{2,1,0:T(4,128)(2,1)S(1)} %reshape.79), channel_id=1, replica_groups=mesh['kv'=8,'tp'=4] {'kv'}, dimensions={0}, use_global_device_ids=true | all-gather | bytes 36864 | tf_op jit(solution)/shard_map/all_gather | solution.py:143
  129.5 1.2 convolution_convert_fusion.3
  130.7 10.3 %psum.35 = bf16[32,512]{1,0:T(8,128)(2,1)S(1)} all-reduce(bf16[32,512]{1,0:T(8,128)(2,1)S(1)} %convolution_convert_fusion.3), channel_id=1, replica_groups=mesh['kv'=8,'tp'=4] {'tp'}, use_global_device_ids=true, to_apply=%region_11.12 | all-reduce | flops 16384 | bytes 65536 | tf_op jit(solution)/shard_map/psum | solution.py:12
  141.2 1.6 convolution_convert_fusion
  142.8 1.6 convolution_convert_fusion.1
  144.4 20.6 %psum.37 = bf16[32]{0:T(256)(128)(2,1)S(1)} all-reduce(bf16[32]{0:T(256)(128)(2,1)S(1)} %get-tuple-element.11), channel_id=1, replica_groups=mesh['kv'=8,'tp'=4] {'kv'}, use_global_device_ids=true, to_apply=%region_14.15 | all-reduce | flops 32 | bytes 128 | tf_op jit(solution)/shard_map/psum | solution.py:157
  165.1 51.4 %all-reduce.13.cloned.1.call-done = (bf16[32,2752]{1,0:T(8,128)(2,1)}, bf16[32,2752]{1,0:T(8,128)(2,1)}) async-done(((bf16[32,2752]{1,0:T(8,128)(2,1)}, bf16[32,2752]{1,0:T(8,128)(2,1)}), (bf16[32,2752]{1,0:T(8,128)(2,1)}, bf16[32,2752]{1,0:T(8,128)(2,1)})) %all-reduce.13.cloned.1.call-update) | async-done | bytes 352272 | tf_op jit(solution)/shard_map/psum | solution.py:156
  216.4 2.6 %convolution_convert_fusion.2 = bf16[32,512]{1,0:T(8,128)(2,1)S(1)} fusion(bf16[2752,512]{1,0:T(8,128)(2,1)} %param.39, bf16[32,2752]{1,0:T(8,128)(2,1)} %get-tuple-element.9, bf16[32,2752]{1,0:T(8,128)(2,1)} %get-tuple-element.10, f32[32]{0:T(128)S(1)} %add_rsqrt_fusion.1), kind=kOutput, calls=%fused_computation.2 | convolution fusion | flops 91074560 | bytes 3203200 | tf_op jit(solution)/shard_map/dot_general | solution.py:160
  219.1 10.3 %psum.39 = bf16[32,512]{1,0:T(8,128)(2,1)S(1)} all-reduce(bf16[32,512]{1,0:T(8,128)(2,1)S(1)} %convolution_convert_fusion.2), channel_id=1, replica_groups=mesh['kv'=8,'tp'=4] {'tp'}, use_global_device_ids=true, to_apply=%region_16.17 | all-reduce | flops 16384 | bytes 65536 | tf_op jit(solution)/shard_map/psum | solution.py:12
  (42 shorter events, 3.0 us)
Async XLA Ops:
  7.2 134.0 %copy-start = (bf16[512,2752]{0,1:T(8,128)(2,1)S(1)}, bf16[512,2752]{0,1:T(8,128)(2,1)}, u32[]{:S(2)}) copy-start(bf16[512,2752]{0,1:T(8,128)(2,1)} %param.38) | copy-start | bytes 8454148
  7.2 15.7 %copy-start.2 = (f32[4,64,2,128]{3,2,1,0:T(2,128)S(1)}, f32[4,64,2,128]{3,2,1,0:T(2,128)}, u32[]{:S(2)}) copy-start(f32[4,64,2,128]{3,2,1,0:T(2,128)} %param.32) | copy-start | bytes 786436
  7.2 85.3 %copy-start.9 = (f32[256]{0:T(256)S(1)}, f32[256]{0:T(256)}, u32[]{:S(2)}) copy-start(f32[256]{0:T(256)} %param.28) | copy-start | bytes 3076
  7.2 85.3 %copy-start.8 = (bf16[16,256]{1,0:T(8,128)(2,1)S(1)}, bf16[16,256]{1,0:T(8,128)(2,1)}, u32[]{:S(2)}) copy-start(bf16[16,256]{1,0:T(8,128)(2,1)} %param.27) | copy-start | bytes 24580
  7.2 91.5 %copy-start.7 = (f32[256]{0:T(256)S(1)}, f32[256]{0:T(256)}, u32[]{:S(2)}) copy-start(f32[256]{0:T(256)} %param.29) | copy-start | bytes 3076
  7.2 84.6 %all-reduce.11.cloned.1.call-start = ((), (), s32[]{:S(2)}) async-start(), calls=%async_computation | async-start | bytes 214016
  10.3 130.7 %copy-start.3 = (bf16[32,512]{1,0:T(8,128)(2,1)S(1)}, bf16[32,512]{1,0:T(8,128)(2,1)}, u32[]{:S(2)}) copy-start(bf16[32,512]{1,0:T(8,128)(2,1)} %param.20) | copy-start | bytes 98308
  12.0 129.1 %copy-start.6 = (f32[512]{0:T(512)S(1)}, f32[512]{0:T(512)}, u32[]{:S(2)}) copy-start(f32[512]{0:T(512)} %param.36) | copy-start | bytes 6148
  17.6 198.9 %all-reduce.13.cloned.1.call-start = ((), (), s32[]{:S(2)}) async-start(), calls=%async_computation.1 | async-start | bytes 720896 | tf_op jit(solution)/shard_map/psum | solution.py:156
  94.2 48.6 %copy-start.5 = (bf16[4,2,128]{2,1,0:T(2,128)(2,1)}, bf16[4,2,128]{2,1,0:T(2,128)(2,1)S(1)}, u32[]{:S(2)}) copy-start(bf16[4,2,128]{2,1,0:T(2,128)(2,1)S(1)} %reshape.74) | copy-start | bytes 6148
  95.0 47.8 %copy-start.4 = (bf16[4,2,256]{2,1,0:T(2,128)(2,1)}, bf16[4,2,256]{2,1,0:T(2,128)(2,1)S(1)}, u32[]{:S(2)}) copy-start(bf16[4,2,256]{2,1,0:T(2,128)(2,1)S(1)} %reshape.75) | copy-start | bytes 12292
  141.0 1.8 copy-start.1
Sparse Core Ops, SparseCore 0:
  17.7 74.0 all-reduce.10
  144.6 71.8 all-reduce.12
where the time goes:
time: 238 us; the launch traced here: 237 us
  waiting for transfers between devices  120 us (50%)
  blocking collectives  71.8 us (30%)
  matrix products  20.1 us (8%)
  between operations  14.8 us (6%)
  other arithmetic  8.62 us (4%)
    unnamed x3, waiting for transfers between devices  68.6 us
    psum x1, waiting for transfers between devices, on_device(): lax.psum(up_part.astype(jnp.bfloat16), 'kv').astype(jnp.float32)  51.4 us
    all_gather x1, blocking collectives, on_device(): lax.all_gather(heads_out, 'kv', axis=0, tiled=True)  30.6 us
    psum x1, blocking collectives, on_device(): lax.psum(mid_squares.astype(jnp.bfloat16), 'kv').astype(jnp.float32)  20.6 us
    psum x2, blocking collectives, across_heads(): lax.psum(partial_value.astype(jnp.bfloat16), 'tp').astype(jnp.float32)  20.5 us
  transfers between devices with their start and end apart: 2, of which 2 were waited for; matrix products, arithmetic and copies ran while one was open for 2% of the time, Pallas kernels for 0%

commit v1 on v0

--- a/solution.py
+++ b/solution.py
@@ -8,8 +8,13 @@
 GATE_TEMP = 16.0
 
 
+def summed_here(array, axis):
+    parts = lax.all_gather(array, axis)
+    return jnp.sum(parts, axis=0)
+
+
 def across_heads(partial_value):
-    return lax.psum(partial_value.astype(jnp.bfloat16), "tp").astype(jnp.float32)
+    return summed_here(partial_value.astype(jnp.bfloat16), "tp").astype(jnp.float32)
 
 
 def block_attention(

time: 238 us -> 228 us (0.958)
  blocking collectives: 71.8 us -> 62.1 us
    psum x2 -> x0, blocking collectives: 20.5 us -> none  [across_heads(): lax.psum(partial_value.astype(jnp.bfloat16), 'tp').astype(jnp.float32)]
    all_gather x0 -> x2, blocking collectives: none -> 10.8 us  [summed_here(): parts = lax.all_gather(array, axis)]
where the time goes in v1:
time: 228 us; the launch traced here: 227 us
  waiting for transfers between devices  120 us (53%)
  blocking collectives  62.1 us (27%)
  matrix products  20.1 us (9%)
  between operations  14.8 us (6%)
  other arithmetic  8.66 us (4%)
    unnamed x3, waiting for transfers between devices  68.6 us
    psum x1, waiting for transfers between devices, on_device(): lax.psum(up_part.astype(jnp.bfloat16), 'kv').astype(jnp.float32)  51.3 us
    all_gather x1, blocking collectives, on_device(): lax.all_gather(heads_out, 'kv', axis=0, tiled=True)  30.6 us
    psum x1, blocking collectives, on_device(): lax.psum(mid_squares.astype(jnp.bfloat16), 'kv').astype(jnp.float32)  20.6 us
    all_gather x2, blocking collectives, summed_here(): parts = lax.all_gather(array, axis)  10.8 us
  transfers between devices with their start and end apart: 2, of which 2 were waited for; matrix products, arithmetic and copies ran while one was open for 2% of the time, Pallas kernels for 0%

profile of v1, /device:TPU:0, one launch (start us, length us, event | category | flops | bytes accessed | tf_op | source)
XLA Modules:
  0.0 227.1 jit_solution(13146004234326946709)
XLA Ops:
  7.3 1.5 fusion.11
  8.8 1.5 convolution_convert_fusion.8
  10.3 1.7 convolution_convert_fusion.7
  12.0 1.7 convolution_convert_fusion.6
  13.8 1.9 convolution_convert_fusion.5
  15.7 1.9 convolution_convert_fusion.4
  18.4 1.2 dynamic-slice
  20.3 2.6 %exponential_multiply_fusion = f32[4,64,2,128]{3,2,1,0:T(2,128)S(1)} fusion(bf16[4,64,2,128]{3,2,1,0:T(2,128)(2,1)} %param.30, f32[4,64,2,128]{3,2,1,0:T(2,128)} %param.32, pred[4,64]{1,0:T(4,128)(4,1)S(1)} %iota_compare_fusion), kind=kOutput, calls=%fused_computation.16 | output fusion | flops 4456448 | bytes 655616 | tf_op jit(solution)/shard_map/block_attention/reduce_window_sum | solution.py:34
  23.2 68.5 %all-reduce.11.cloned.1.call-done = (bf16[32,512]{1,0:T(8,128)(2,1)}, bf16[32]{0:T(256)(128)(2,1)}, bf16[32,256]{1,0:T(8,128)(2,1)}, bf16[32,16]{1,0:T(8,128)(2,...) async-done(((bf16[32,512]{1,0:T(8,128)(2,1)}, bf16[32]{0:T(256)(128)(2,1)}, bf16[32,256]{1,0:T(8,128)(2,1)}, bf16[32,16]{1,0:T(8,128)(2,1)}, ...) | async-done | bytes 99408
  91.8 0.7 fusion.36
  92.5 0.9 fusion.29
  93.4 0.8 multiply_convert_fusion.4
  94.2 0.8 multiply_convert_fusion.3
  95.6 1.8 fusion.41
  97.5 1.1 fusion.1
  98.9 30.6 %all-gather.2 = bf16[8,4,512]{2,1,0:T(4,128)(2,1)S(1)} all-gather(bf16[1,4,512]{2,1,0:T(4,128)(2,1)S(1)} %reshape.81), channel_id=1, replica_groups=mesh['kv'=8,'tp'=4] {'kv'}, dimensions={0}, use_global_device_ids=true | all-gather | bytes 36864 | tf_op jit(solution)/shard_map/all_gather | solution.py:148
  129.5 1.2 convolution_convert_fusion.3
  130.7 5.4 %all-gather = bf16[128,512]{1,0:T(8,128)(2,1)S(1)} all-gather(bf16[32,512]{1,0:T(8,128)(2,1)S(1)} %convolution_convert_fusion.3), channel_id=2, replica_groups=mesh['kv'=8,'tp'=4] {'tp'}, dimensions={0}, use_global_device_ids=true | all-gather | bytes 163840 | tf_op jit(solution)/shard_map/all_gather | solution.py:12
  136.3 1.6 convolution_convert_fusion
  138.0 1.6 convolution_convert_fusion.1
  139.6 20.6 %psum.22 = bf16[32]{0:T(256)(128)(2,1)S(1)} all-reduce(bf16[32]{0:T(256)(128)(2,1)S(1)} %get-tuple-element.11), channel_id=1, replica_groups=mesh['kv'=8,'tp'=4] {'kv'}, use_global_device_ids=true, to_apply=%region_14.15 | all-reduce | flops 32 | bytes 128 | tf_op jit(solution)/shard_map/psum | solution.py:162
  160.2 51.3 %all-reduce.13.cloned.1.call-done = (bf16[32,2752]{1,0:T(8,128)(2,1)}, bf16[32,2752]{1,0:T(8,128)(2,1)}) async-done(((bf16[32,2752]{1,0:T(8,128)(2,1)}, bf16[32,2752]{1,0:T(8,128)(2,1)}), (bf16[32,2752]{1,0:T(8,128)(2,1)}, bf16[32,2752]{1,0:T(8,128)(2,1)})) %all-reduce.13.cloned.1.call-update) | async-done | bytes 352272 | tf_op jit(solution)/shard_map/psum | solution.py:161
  211.6 2.6 %convolution_convert_fusion.2 = bf16[32,512]{1,0:T(8,128)(2,1)S(1)} fusion(bf16[2752,512]{1,0:T(8,128)(2,1)} %param.39, bf16[32,2752]{1,0:T(8,128)(2,1)} %get-tuple-element.9, bf16[32,2752]{1,0:T(8,128)(2,1)} %get-tuple-element.10, f32[32]{0:T(128)S(1)} %add_rsqrt_fusion.1), kind=kOutput, calls=%fused_computation.2 | convolution fusion | flops 91074560 | bytes 3203200 | tf_op jit(solution)/shard_map/dot_general | solution.py:165
  214.2 5.4 %all-gather.1 = bf16[128,512]{1,0:T(8,128)(2,1)S(1)} all-gather(bf16[32,512]{1,0:T(8,128)(2,1)S(1)} %convolution_convert_fusion.2), channel_id=3, replica_groups=mesh['kv'=8,'tp'=4] {'tp'}, dimensions={0}, use_global_device_ids=true | all-gather | bytes 163840 | tf_op jit(solution)/shard_map/all_gather | solution.py:12
  (44 shorter events, 3.0 us)
Async XLA Ops:
  7.2 129.1 %copy-start = (bf16[512,2752]{0,1:T(8,128)(2,1)S(1)}, bf16[512,2752]{0,1:T(8,128)(2,1)}, u32[]{:S(2)}) copy-start(bf16[512,2752]{0,1:T(8,128)(2,1)} %param.38) | copy-start | bytes 8454148
  7.2 15.7 %copy-start.2 = (f32[4,64,2,128]{3,2,1,0:T(2,128)S(1)}, f32[4,64,2,128]{3,2,1,0:T(2,128)}, u32[]{:S(2)}) copy-start(f32[4,64,2,128]{3,2,1,0:T(2,128)} %param.32) | copy-start | bytes 786436
  7.2 85.3 %copy-start.9 = (f32[256]{0:T(256)S(1)}, f32[256]{0:T(256)}, u32[]{:S(2)}) copy-start(f32[256]{0:T(256)} %param.28) | copy-start | bytes 3076
  7.2 85.3 %copy-start.8 = (bf16[16,256]{1,0:T(8,128)(2,1)S(1)}, bf16[16,256]{1,0:T(8,128)(2,1)}, u32[]{:S(2)}) copy-start(bf16[16,256]{1,0:T(8,128)(2,1)} %param.27) | copy-start | bytes 24580
  7.2 91.5 %copy-start.7 = (f32[256]{0:T(256)S(1)}, f32[256]{0:T(256)}, u32[]{:S(2)}) copy-start(f32[256]{0:T(256)} %param.29) | copy-start | bytes 3076
  7.2 84.6 %all-reduce.11.cloned.1.call-start = ((), (), s32[]{:S(2)}) async-start(), calls=%async_computation | async-start | bytes 214016
  12.0 124.1 %copy-start.3 = (bf16[32,512]{1,0:T(8,128)(2,1)S(1)}, bf16[32,512]{1,0:T(8,128)(2,1)}, u32[]{:S(2)}) copy-start(bf16[32,512]{1,0:T(8,128)(2,1)} %param.20) | copy-start | bytes 98308
  13.8 122.5 %copy-start.6 = (f32[512]{0:T(512)S(1)}, f32[512]{0:T(512)}, u32[]{:S(2)}) copy-start(f32[512]{0:T(512)} %param.36) | copy-start | bytes 6148
  17.6 194.0 %all-reduce.13.cloned.1.call-start = ((), (), s32[]{:S(2)}) async-start(), calls=%async_computation.1 | async-start | bytes 720896 | tf_op jit(solution)/shard_map/psum | solution.py:161
  94.2 43.7 %copy-start.5 = (bf16[4,2,128]{2,1,0:T(2,128)(2,1)}, bf16[4,2,128]{2,1,0:T(2,128)(2,1)S(1)}, u32[]{:S(2)}) copy-start(bf16[4,2,128]{2,1,0:T(2,128)(2,1)S(1)} %reshape.74) | copy-start | bytes 6148
  95.0 42.9 %copy-start.4 = (bf16[4,2,256]{2,1,0:T(2,128)(2,1)}, bf16[4,2,256]{2,1,0:T(2,128)(2,1)S(1)}, u32[]{:S(2)}) copy-start(bf16[4,2,256]{2,1,0:T(2,128)(2,1)S(1)} %reshape.75) | copy-start | bytes 12292
  136.2 1.8 copy-start.1
Sparse Core Ops, SparseCore 0:
  17.7 74.0 all-reduce.10
  139.7 71.7 all-reduce.12
